TPU v7x, 32 devices: a whole 2x2x4 slice. The times are simulated.
32 devices in a mesh: sp: 4 (over z), fs: 4 (over y, x), tp: 2 (over core).
Axes of the slice: x: 2, y: 2, z: 4, core: 2. Of those that a mesh axis runs over, the one named last changes fastest.
Arguments:
- tokens: bfloat16 [4096, 2048], P(('fs', 'sp', 'tp')), parts along dimension 0, may hold values from -6 to 6
- norm_gain: float32 [2048], replicated, may hold values from 0.1 to 1.9
- recurrent_input: bfloat16 [2048, 1024], P(None, 'tp'), may hold values from -0.125 to 0.125
- recurrent_gate: bfloat16 [2048, 1024], P(None, 'tp'), may hold values from -0.125 to 0.125
- attention_gate: bfloat16 [2048, 1024], P(None, 'tp'), may hold values from -0.125 to 0.125
- query_proj: bfloat16 [2048, 1536], P(None, 'tp'), may hold values from -0.125 to 0.125
- latent_down: bfloat16 [2048, 512], P(None, 'tp'), may hold values from -0.125 to 0.125
- rope_key_down: bfloat16 [2048, 64], replicated, may hold values from -0.125 to 0.125
- conv_kernel: float32 [4, 1024], P(None, 'tp'), may hold values from -3 to 3
- recurrence_gate_blocks: bfloat16 [16, 64, 64], P('tp'), may hold values from -0.75 to 0.75
- input_gate_blocks: bfloat16 [16, 64, 64], P('tp'), may hold values from -0.75 to 0.75
- decay_rate: float32 [1024], P('tp'), as said below
- decay_shift: float32 [4096], P(('fs', 'sp')), parts along dimension 0, may hold values from -2 to 0, as said below
- initial_state: float32 [4096], P(('fs', 'tp')), parts along dimension 0, may hold values from -6 to 6
- latent_gain: float32 [512], replicated, may hold values from 0.1 to 1.9
- latent_up: bfloat16 [512, 2048], P(None, 'tp'), may hold values from -0.25 to 0.25
- query_gain: float32 [192], replicated, may hold values from 0.4 to 250, as said below
- recurrent_output: bfloat16 [1024, 2048], P('tp'), may hold values from -0.25 to 0.25
- attention_output: bfloat16 [1024, 2048], P('tp'), may hold values from -0.25 to 0.25
Outputs:
- mixed_output: bfloat16 [4096, 2048], P(('fs', 'sp', 'tp')), parts along dimension 0
There are 4 independent parts, one for each index of `fs`. A program takes and returns all parts, laid end to end along the dimension named above; an argument that names none is the same for every part. Nothing has to cross between parts.
Inputs may be any that keep to these rules, and one draw needn't show every extreme that they name: `decay_rate`: positive. `decay_shift`: negative. `query_gain`: positive.
All inputs are finite; a program needn't handle non-finite values.
Results may differ from a plain program's by a relative error of at most 0.03.
The roundings to bfloat16 on the way count: a program that leaves them out, or rounds other values in their place, can miss the bound.
Values may be sent and summed in bfloat16 or wider, within the bound.
A program may use at most 128 MiB of HBM per device.

v0:
```python
import math

import jax
import jax.numpy as jnp
from jax import lax
from jax.sharding import PartitionSpec as P

EPS = 1e-06
RECURRENT_SCALE = 8.0
THETA = 10000.0


def from_behind(block, axis, distance):
    devices = range(lax.axis_size(axis))
    route = [(i - distance, i) for i in devices if i - distance in devices]
    return lax.ppermute(block, axis, route)


def prefix(part, axis, combine, identity):
    place = lax.axis_index(axis)
    gathered = jax.tree.map(lambda a: lax.all_gather(a, axis), part)
    state = jax.tree.map(lambda a, e: jnp.zeros_like(a) + jnp.asarray(e, a.dtype), part, identity)

    def one(hop, state):
        return combine(
            state, jax.tree.map(lambda a: lax.dynamic_index_in_dim(a, hop, 0, False), gathered)
        )

    return lax.fori_loop(0, place, one, state)


def rotate_half(values, token_positions):
    half_width = values.shape[-1] // 2
    inv_freq = 1.0 / THETA ** (
        jnp.arange(0, 2 * half_width, 2, dtype=jnp.float32) / (2 * half_width)
    )
    angles = token_positions.astype(jnp.float32)[:, None] * inv_freq[None, :]
    cosine = jnp.cos(angles)
    sine_part = jnp.sin(angles)
    if values.ndim == 3:
        cosine = cosine[:, None, :]
        sine_part = sine_part[:, None, :]
    first_half = values[..., :half_width]
    second_half = values[..., half_width:]
    return jnp.concatenate(
        [
            first_half * cosine - second_half * sine_part,
            first_half * sine_part + second_half * cosine,
        ],
        axis=-1,
    )


def rms_scaled(values, gain_vec):
    return values * lax.rsqrt(jnp.mean(values * values, axis=-1, keepdims=True) + EPS) * gain_vec


def linear_step(earlier, later_part):
    return (earlier[0] * later_part[0], later_part[0] * earlier[1] + later_part[1])


def body(
    tokens,
    norm_gain,
    recurrent_input,
    recurrent_gate,
    attention_gate,
    query_proj,
    latent_down,
    rope_key_down,
    conv_kernel,
    recurrence_gate_blocks,
    input_gate_blocks,
    decay_rate,
    decay_shift,
    initial_state,
    latent_gain,
    latent_up,
    query_gain,
    recurrent_output,
    attention_output,
):
    tp_count = lax.axis_size("tp")
    sp_count = lax.axis_size("sp")
    sp_place = lax.axis_index("sp")
    tp_place = lax.axis_index("tp")
    channel_width = recurrent_input.shape[1]
    value_width = attention_gate.shape[1]
    query_width = query_proj.shape[1]
    latent_width = latent_down.shape[1]
    rope_width = rope_key_down.shape[1]
    head_dim = query_gain.shape[0]
    nope_width = head_dim - rope_width
    local_heads = query_width // head_dim
    head_value = value_width // local_heads
    joined_weight = jnp.concatenate(
        [recurrent_input, recurrent_gate, attention_gate, query_proj, latent_down, rope_key_down],
        axis=1,
    )
    normed = rms_scaled(
        lax.all_gather(tokens, "tp", axis=0, tiled=True).astype(jnp.float32), norm_gain
    ).astype(jnp.bfloat16)
    projected = jnp.dot(normed, joined_weight, preferred_element_type=jnp.float32).astype(
        jnp.bfloat16
    )
    local_tokens = projected.shape[0]
    split_points = []
    running_total = 0
    for width_part in [channel_width, channel_width, value_width, query_width, latent_width]:
        running_total += width_part
        split_points.append(running_total)
    recur_signal, recur_gate_pre, attention_pre, query_raw, latent_local, rope_raw = jnp.split(
        projected, split_points, axis=1
    )
    token_positions = sp_place * local_tokens + jnp.arange(local_tokens, dtype=jnp.int32)
    taps = conv_kernel.shape[0]
    conv_rim = from_behind(recur_signal[local_tokens - taps + 1 :], "sp", 1)
    extended = jnp.concatenate([conv_rim, recur_signal], axis=0).astype(jnp.float32)
    conv_sum = conv_kernel[0] * extended[0:local_tokens]
    for tap_index in range(1, taps):
        conv_sum = (
            conv_sum + conv_kernel[tap_index] * extended[tap_index : tap_index + local_tokens]
        )
    conv_out = conv_sum.astype(jnp.bfloat16)
    block_size = recurrence_gate_blocks.shape[1]
    grouped = conv_out.reshape(local_tokens, channel_width // block_size, block_size)
    recur_rate = jax.nn.sigmoid(
        jnp.einsum(
            "tbi,bij->tbj", grouped, recurrence_gate_blocks, preferred_element_type=jnp.float32
        ).reshape(local_tokens, channel_width)
    )
    input_rate = jax.nn.sigmoid(
        jnp.einsum(
            "tbi,bij->tbj", grouped, input_gate_blocks, preferred_element_type=jnp.float32
        ).reshape(local_tokens, channel_width)
    )
    log_decay = -RECURRENT_SCALE * recur_rate * decay_rate + decay_shift[:, None]
    decay = jnp.exp(log_decay)
    driven = jnp.sqrt(-jnp.expm1(2.0 * log_decay)) * input_rate * conv_out.astype(jnp.float32)
    decay_prod, zero_state = lax.associative_scan(linear_step, (decay, driven), axis=0)
    carry_decay, carry_state = prefix(
        (decay_prod[-1], zero_state[-1]),
        "sp",
        linear_step,
        (jnp.ones_like(initial_state), jnp.zeros_like(initial_state)),
    )
    incoming = carry_decay * initial_state + carry_state
    states = zero_state + decay_prod * incoming
    recur_out = (states * jax.nn.silu(recur_gate_pre.astype(jnp.float32))).astype(jnp.bfloat16)
    query_rows = rms_scaled(
        query_raw.astype(jnp.float32).reshape(local_tokens, local_heads, head_dim), query_gain
    )
    query_rows = jnp.concatenate(
        [query_rows[..., :nope_width], rotate_half(query_rows[..., nope_width:], token_positions)],
        axis=-1,
    ).astype(jnp.bfloat16)
    query_nope = query_rows[..., :nope_width]
    query_rope = query_rows[..., nope_width:]
    rope_share = rope_width // tp_count
    rotary_portion = lax.dynamic_slice_in_dim(rope_raw, tp_place * rope_share, rope_share, 1)
    outgoing = jnp.concatenate([latent_local, rotary_portion], axis=1)
    arrived = lax.all_gather(outgoing, ("sp", "tp"), axis=1, tiled=True)
    grid_view = arrived.reshape(local_tokens, sp_count, tp_count, latent_width + rope_share)
    key_count = local_tokens * sp_count
    latent_all = grid_view[..., :latent_width].reshape(key_count, tp_count * latent_width)
    rope_all = grid_view[..., latent_width:].reshape(key_count, rope_width)
    key_positions = (
        jnp.arange(sp_count, dtype=jnp.int32)[None, :] * local_tokens
        + jnp.arange(local_tokens, dtype=jnp.int32)[:, None]
    ).reshape(key_count)
    normed_latent = rms_scaled(latent_all.astype(jnp.float32), latent_gain).astype(jnp.bfloat16)
    expanded = jnp.dot(normed_latent, latent_up, preferred_element_type=jnp.float32).astype(
        jnp.bfloat16
    )
    key_rope = rotate_half(rope_all.astype(jnp.float32), key_positions).astype(jnp.bfloat16)
    head_keys = expanded.reshape(key_count, local_heads, nope_width + head_value)
    key_nope = head_keys[..., :nope_width]
    key_values = head_keys[..., nope_width:]
    key_group = math.gcd(sp_count, 4)
    block_keys = local_tokens * key_group
    block_total = key_count // block_keys
    score_scale = head_dim ** (-0.5)

    def online_step(block_index, carried):
        running_max, total_weight, weighted = carried
        begin_key = block_index * block_keys
        nope_block = lax.dynamic_slice_in_dim(key_nope, begin_key, block_keys, 0)
        rope_block = lax.dynamic_slice_in_dim(key_rope, begin_key, block_keys, 0)
        pos_block = lax.dynamic_slice_in_dim(key_positions, begin_key, block_keys, 0)
        value_block = lax.dynamic_slice_in_dim(key_values, begin_key, block_keys, 0)
        scores = jnp.einsum(
            "thd,khd->htk", query_nope, nope_block, preferred_element_type=jnp.float32
        )
        scores = scores + jnp.einsum(
            "thr,kr->htk", query_rope, rope_block, preferred_element_type=jnp.float32
        )
        scores = scores * score_scale
        allowed = pos_block[None, :] <= token_positions[:, None]
        scores = jnp.where(allowed[None], scores, -jnp.inf)
        new_max = jnp.maximum(running_max, jnp.max(scores, axis=-1))
        rescale = jnp.exp(running_max - new_max)
        weights = jnp.exp(scores - new_max[..., None])
        block_weighted = jnp.einsum(
            "htk,khd->thd",
            weights.astype(jnp.bfloat16),
            value_block,
            preferred_element_type=jnp.float32,
        )
        weighted = weighted * jnp.transpose(rescale)[:, :, None] + block_weighted
        total_weight = total_weight * rescale + jnp.sum(weights, axis=-1)
        return (new_max, total_weight, weighted)

    start_sums = (
        jnp.full((local_heads, local_tokens), -jnp.inf, jnp.float32),
        jnp.zeros((local_heads, local_tokens), jnp.float32),
        jnp.zeros((local_tokens, local_heads, head_value), jnp.float32),
    )
    row_max, total_weight, weighted = lax.fori_loop(0, block_total, online_step, start_sums)
    attended = weighted / jnp.transpose(total_weight)[:, :, None]
    attention_out = (
        attended.reshape(local_tokens, value_width) * jax.nn.silu(attention_pre.astype(jnp.float32))
    ).astype(jnp.bfloat16)
    return lax.psum_scatter(
        (
            jnp.dot(recur_out, recurrent_output, preferred_element_type=jnp.float32)
            + jnp.dot(attention_out, attention_output, preferred_element_type=jnp.float32)
        ).astype(jnp.bfloat16),
        "tp",
        scatter_dimension=0,
        tiled=True,
    )


def solution(mesh):
    return jax.shard_map(
        body,
        mesh=mesh,
        in_specs=(
            P(("fs", "sp", "tp"), None),
            P(),
            P(None, "tp"),
            P(None, "tp"),
            P(None, "tp"),
            P(None, "tp"),
            P(None, "tp"),
            P(),
            P(None, "tp"),
            P("tp", None, None),
            P("tp", None, None),
            P("tp"),
            P(("fs", "sp")),
            P(("fs", "tp")),
            P(),
            P(None, "tp"),
            P(),
            P("tp", None),
            P("tp", None),
        ),
        out_specs=P(("fs", "sp", "tp"), None),
        check_vma=False,
    )
```

profile of v0, /device:TPU:0, one launch (start us, length us, event | category | flops | bytes accessed | tf_op | source)
XLA Modules:
  0.0 521.1 jit_solution(13550324837201911915)
XLA Ops:
  26.6 8.9 %convolution_convert_fusion = bf16[256,2624]{0,1:T(8,128)(2,1)S(1)} fusion(bf16[2048,2624]{1,0:T(8,128)(2,1)} %constant_dynamic-update-slice_fusion, bf16[256,2048]{1,0:T(8,128)(2,1)} %all-gather.5.cloned.1.call-done, f32[2048]{0:T(1024)S(1)} %copy-done.34, f32[256]{0:T(256)S(1)} %add_rsqrt_fusion.2), kind=kOutput, calls=%fused_computation.7 | convolution fusion | flops 2754232320 | bytes 13149184 | tf_op jit(solution)/shard_map/dot_general | solution.py:103
  38.6 5.1 collective-permute-start
  52.0 12.1 %slice.365 = f32[127,512]{0,1:T(8,128)} slice(f32[256,512]{0,1:T(8,128)S(1)} %get-tuple-element.95), slice={[2:256:2], [0:512:1]} | slice | bytes 520192 | tf_op jit(solution)/shard_map/slice | solution.py:140
  64.1 11.7 %slice.311 = f32[128,512]{0,1:T(8,128)S(1)} slice(f32[256,512]{0,1:T(8,128)S(1)} %get-tuple-element.95), slice={[1:256:2], [0:512:1]} | slice | bytes 524288 | tf_op jit(solution)/shard_map/slice | solution.py:140
  75.9 12.1 %slice.308 = f32[127,512]{0,1:T(8,128)} slice(f32[256,512]{0,1:T(8,128)S(1)} %get-tuple-element.96), slice={[2:256:2], [0:512:1]} | slice | bytes 520192 | tf_op jit(solution)/shard_map/slice | solution.py:140
  88.0 12.4 %slice.309 = f32[128,512]{0,1:T(8,128)} slice(f32[256,512]{0,1:T(8,128)S(1)} %get-tuple-element.96), slice={[1:256:2], [0:512:1]} | slice | bytes 524288 | tf_op jit(solution)/shard_map/slice | solution.py:140
  100.3 12.2 %slice.310 = f32[128,512]{0,1:T(8,128)} slice(f32[256,512]{0,1:T(8,128)S(1)} %get-tuple-element.95), slice={[0:255:2], [0:512:1]} | slice | bytes 524288 | tf_op jit(solution)/shard_map/slice | solution.py:140
  112.5 12.2 %slice.313 = f32[128,512]{0,1:T(8,128)} slice(f32[256,512]{0,1:T(8,128)S(1)} %get-tuple-element.96), slice={[0:255:2], [0:512:1]} | slice | bytes 524288 | tf_op jit(solution)/shard_map/slice | solution.py:140
  125.9 6.4 %slice.317 = f32[64,512]{0,1:T(8,128)S(1)} slice(f32[128,512]{0,1:T(8,128)S(1)} %get-tuple-element.134), slice={[1:128:2], [0:512:1]} | slice | bytes 262144 | tf_op jit(solution)/shard_map/slice | solution.py:140
  132.4 6.5 %slice.316 = f32[64,512]{0,1:T(8,128)} slice(f32[128,512]{0,1:T(8,128)S(1)} %get-tuple-element.134), slice={[0:127:2], [0:512:1]} | slice | bytes 262144 | tf_op jit(solution)/shard_map/slice | solution.py:140
  138.9 7.1 %slice.315 = f32[64,512]{0,1:T(8,128)} slice(f32[128,512]{0,1:T(8,128)S(1)} %get-tuple-element.135), slice={[1:128:2], [0:512:1]} | slice | bytes 262144 | tf_op jit(solution)/shard_map/slice | solution.py:140
  146.0 6.5 %slice.319 = f32[64,512]{0,1:T(8,128)} slice(f32[128,512]{0,1:T(8,128)S(1)} %get-tuple-element.135), slice={[0:127:2], [0:512:1]} | slice | bytes 262144 | tf_op jit(solution)/shard_map/slice | solution.py:140
  153.7 3.7 slice.361
  157.4 3.8 slice.323
  161.2 3.7 slice.320
  164.9 3.8 slice.321
  168.7 3.7 slice.322
  172.4 3.7 slice.325
  248.4 6.8 %slice.363 = f32[63,512]{0,1:T(8,128)} slice(f32[128,512]{0,1:T(8,128)S(1)} %get-tuple-element.134), slice={[2:128:2], [0:512:1]} | slice | bytes 258048 | tf_op jit(solution)/shard_map/slice | solution.py:140
  255.3 6.8 %slice.314 = f32[63,512]{0,1:T(8,128)} slice(f32[128,512]{0,1:T(8,128)S(1)} %get-tuple-element.135), slice={[2:128:2], [0:512:1]} | slice | bytes 258048 | tf_op jit(solution)/shard_map/slice | solution.py:140
  363.9 5.3 %pad.111 = f32[128,512]{0,1:T(8,128)S(1)} pad(f32[64,512]{0,1:T(8,128)} %add.379, f32[]{:T(128)} %constant.25.clone.1), padding=1_0_1x0_0_0 | pad | bytes 393220 | tf_op jit(solution)/shard_map/pad | solution.py:140
  369.2 4.6 pad.125
  382.6 4.3 pad.110
  386.9 5.3 %pad.127 = f32[128,512]{0,1:T(8,128)S(1)} pad(f32[64,512]{0,1:T(8,128)} %add.389, f32[]{:T(128)} %constant.25.clone.1), padding=1_0_1x0_0_0 | pad | bytes 393220 | tf_op jit(solution)/shard_map/pad | solution.py:140
  393.3 4.7 pad.126
  401.5 8.6 %pad.128 = f32[256,512]{0,1:T(8,128)S(1)} pad(f32[128,512]{0,1:T(8,128)S(1)} %pad_maximum_fusion.10, f32[]{:T(128)} %constant.25.clone.1), padding=0_1_1x0_0_0 | pad | bytes 786436 | tf_op jit(solution)/shard_map/pad | solution.py:140
  410.1 9.8 %pad.129 = f32[256,512]{0,1:T(8,128)S(1)} pad(f32[128,512]{0,1:T(8,128)} %add.390, f32[]{:T(128)} %constant.25.clone.1), padding=1_0_1x0_0_0 | pad | bytes 786436 | tf_op jit(solution)/shard_map/pad | solution.py:140
  421.7 11.2 %pad.112 = f32[256,512]{0,1:T(8,128)} pad(f32[128,512]{0,1:T(8,128)} %pad_maximum_fusion.3, f32[]{:T(128)} %constant.25.clone.1), padding=0_1_1x0_0_0 | pad | bytes 786436 | tf_op jit(solution)/shard_map/pad | solution.py:140
  432.9 11.3 %pad.113 = f32[256,512]{0,1:T(8,128)} pad(f32[128,512]{0,1:T(8,128)} %add.381, f32[]{:T(128)} %constant.25.clone.1), padding=1_0_1x0_0_0 | pad | bytes 786436 | tf_op jit(solution)/shard_map/pad | solution.py:140
  444.5 12.1 %all-gather = f32[4,1,512]{2,1,0:T(1,128)S(1)} all-gather(f32[1,1,512]{2,1,0:T(1,128)S(1)} %bitcast.121), channel_id=1, replica_groups=mesh['sp'=4,'fs'=4,'tp'=2] {'sp'}, dimensions={0}, use_global_device_ids=true | all-gather | bytes 10240 | tf_op jit(solution)/shard_map/all_gather | solution.py:21
  457.9 11.9 %all-gather.1 = f32[4,1,512]{2,1,0:T(1,128)S(1)} all-gather(f32[1,1,512]{2,1,0:T(1,128)S(1)} %bitcast.122), channel_id=1, replica_groups=mesh['sp'=4,'fs'=4,'tp'=2] {'sp'}, dimensions={0}, use_global_device_ids=true | all-gather | bytes 10240 | tf_op jit(solution)/shard_map/all_gather | solution.py:21
  506.9 7.2 %reduce-scatter.2.cloned.1.call-done = bf16[128,2048]{1,0:T(8,128)(2,1)} async-done(((bf16[256,2048]{1,0:T(8,128)(2,1)}), bf16[128,2048]{1,0:T(8,128)(2,1)}) %reduce-scatter.2.cloned.1.call-update) | async-done | bytes 524304 | tf_op jit(solution)/shard_map/reduce_scatter | solution.py:223
  (249 shorter events, 261.1 us)
Async XLA Ops:
  6.5 463.4 %copy-start = (bf16[512,2048]{1,0:T(8,128)(2,1)S(1)}, bf16[512,2048]{1,0:T(8,128)(2,1)}, u32[]{:S(2)}) copy-start(bf16[512,2048]{1,0:T(8,128)(2,1)} %param.38) | copy-start | bytes 6291460
  6.5 18.5 %all-gather.5.cloned.1.call-start = ((), (), s32[]{:S(2)}) async-start(), calls=%async_computation.1 | async-start | bytes 1572864 | tf_op jit(solution)/shard_map/all_gather | solution.py:101
  7.3 466.1 %all-gather.7.cloned.1.call-start = ((), (), s32[]{:S(2)}) async-start(), calls=%async_computation.2 | async-start | bytes 1327104 | tf_op jit(solution)/shard_map/all_gather | solution.py:162
  7.3 8.9 %copy-start.27 = (f32[32]{0:T(128)}, f32[32]{0:T(128)S(1)}, u32[]{:S(2)}) copy-start(f32[32]{0:T(128)S(1)} %negate_power_fusion) | copy-start | bytes 388
  7.3 3.2 copy-start.23
  7.4 3.5 copy-start.26
  7.4 3.5 copy-start.29
  17.5 3.5 copy-start.9
  21.0 2.0 copy-start.18
  23.0 3.6 copy-start.34
  35.5 2.2 copy-start.13
  38.6 9.6 %copy-start.19 = (f32[256,32]{1,0:T(8,128)S(1)}, f32[256,32]{1,0:T(8,128)}, u32[]{:S(2)}) copy-start(f32[256,32]{1,0:T(8,128)} %get-tuple-element.140) | copy-start | bytes 98308
  38.6 9.6 %copy-start.20 = (f32[256,32]{1,0:T(8,128)S(1)}, f32[256,32]{1,0:T(8,128)}, u32[]{:S(2)}) copy-start(f32[256,32]{1,0:T(8,128)} %get-tuple-element.141) | copy-start | bytes 98308
  38.6 10.7 %collective-permute-start = (bf16[3,512]{0,1:T(8,128)(2,1)}, bf16[3,512]{0,1:T(8,128)(2,1)S(1)}, u32[]{:S(2)}, u32[]{:S(2)}) collective-permute-start(bf16[3,512]{0,1:T(8,128)(2,1)} %slice.392), channel_id=1, source_target_pairs={{0,8},{8,16},{16,24},{1,9},{9,17},{17,25},{2,10},{10,18},{18,26},{... | collective-permute-start | bytes 9224 | tf_op jit(solution)/shard_map/ppermute | solution.py:16
  46.1 468.1 %reduce-scatter.2.cloned.1.call-start = ((), (), s32[]{:S(2)}) async-start(), calls=%async_computation.3 | async-start | bytes 1572864 | tf_op jit(solution)/shard_map/reduce_scatter | solution.py:223
  47.3 2.1 slice-start
  52.0 60.5 %copy-start.7 = (f32[256,512]{0,1:T(8,128)}, f32[256,512]{0,1:T(8,128)S(1)}, u32[]{:S(2)}) copy-start(f32[256,512]{0,1:T(8,128)S(1)} %get-tuple-element.95) | copy-start | bytes 1572868
  52.0 73.9 %copy-start.8 = (f32[256,512]{0,1:T(8,128)}, f32[256,512]{0,1:T(8,128)S(1)}, u32[]{:S(2)}) copy-start(f32[256,512]{0,1:T(8,128)S(1)} %get-tuple-element.96) | copy-start | bytes 1572868
  230.8 1.5 copy-start.6
  332.6 3.9 copy-start.2
  346.2 7.1 %copy-start.10 = (f32[32,512]{0,1:T(8,128)S(1)}, f32[32,512]{0,1:T(8,128)}, u32[]{:S(2)}) copy-start(f32[32,512]{0,1:T(8,128)} %pad.107) | copy-start | bytes 196612
  398.1 3.3 copy-start.17
  399.5 20.4 %copy-start.16 = (f32[1,512]{0,1:T(8,128)S(1)}, f32[1,512]{0,1:T(8,128)}, u32[]{:S(2)}) copy-start(f32[1,512]{0,1:T(8,128)} %slice.397) | copy-start | bytes 6148
  419.9 50.0 %copy-start.30 = (f32[512]{0:T(512)S(1)}, f32[512]{0:T(512)}, u32[]{:S(2)}) copy-start(f32[512]{0:T(512)} %param.34) | copy-start | bytes 6148
  479.4 4.5 copy-start.35
  484.0 4.7 copy-start.4
  494.4 2.4 copy-start.24
  494.4 2.4 copy-start.28
  494.5 3.0 copy-start.15
  500.9 1.6 copy-start.22
  502.5 2.0 copy-start.1
  502.5 2.6 copy-start.12
  (9 other events, 9.8 us)
Sparse Core Ops, SparseCore 0:
  8.9 11.8 all-gather.4
  46.2 22.9 all-gather.6
  507.1 7.0 reduce-scatter.1
where the time goes:
time: 531 us; the launch traced here: 521 us
  local copies, waits for them, and re-layouts  366 us (69%)
  other arithmetic  77.6 us (15%)
  matrix products  25.5 us (5%)
  blocking collectives  24 us (5%)
  between operations  14.2 us (3%)
  waiting for transfers between devices  7.96 us (1%)
  starting transfers between devices  5.64 us (1%)
    slice x42, local copies, waits for them, and re-layouts, body(): lax.associative_scan(linear_step, (decay, driven), axis=0)  199 us
    pad x28, local copies, waits for them, and re-layouts, body(): lax.associative_scan(linear_step, (decay, driven), axis=0)  121 us
    unnamed x91, local copies, waits for them, and re-layouts  30.7 us
    all_gather x2, blocking collectives, prefix(): gathered = jax.tree.map(lambda a: lax.all_gather(a, axis), part)  24 us
    add x15, other arithmetic, linear_step(): later_part[0] * earlier[1] + later_part[1]  19.9 us
    add x13, other arithmetic, body(): lax.associative_scan(linear_step, (decay, driven), axis=0)  19 us
    concatenate x14, other arithmetic, body(): lax.associative_scan(linear_step, (decay, driven), axis=0)  14.1 us
  transfers between devices with their start and end apart: 4, of which 1 were waited for; matrix products, arithmetic and copies ran while one was open for 81% of the time, Pallas kernels for 0%

commit v1 on v0

--- a/solution.py
+++ b/solution.py
@@ -3,6 +3,8 @@
 import jax
 import jax.numpy as jnp
 from jax import lax
+from jax.experimental import pallas as pl
+from jax.experimental.pallas import tpu as pltpu
 from jax.sharding import PartitionSpec as P
 
 EPS = 1e-06
@@ -16,17 +18,61 @@
     return lax.ppermute(block, axis, route)
 
 
-def prefix(part, axis, combine, identity):
-    place = lax.axis_index(axis)
-    gathered = jax.tree.map(lambda a: lax.all_gather(a, axis), part)
-    state = jax.tree.map(lambda a, e: jnp.zeros_like(a) + jnp.asarray(e, a.dtype), part, identity)
-
-    def one(hop, state):
-        return combine(
-            state, jax.tree.map(lambda a: lax.dynamic_index_in_dim(a, hop, 0, False), gathered)
-        )
-
-    return lax.fori_loop(0, place, one, state)
+def expm1_neg(y):
+    small = y * (1.0 + y * (0.5 + y * (1.0 / 6 + y * (1.0 / 24 + y * (1.0 / 120 + y / 720)))))
+    return jnp.where(y > -0.35, small, jnp.exp(y) - 1.0)
+
+
+def block_diagonal(scratch, blocks_ref, first):
+    size = blocks_ref.shape[1]
+    scratch[...] = jnp.zeros_like(scratch)
+    for k in range(scratch.shape[0] // size):
+        scratch[k * size : (k + 1) * size, k * size : (k + 1) * size] = blocks_ref[first + k]
+    return scratch[...]
+
+
+def scan_rows(decay, state):
+    rows = decay.shape[0]
+    row = lax.broadcasted_iota(jnp.int32, decay.shape, 0)
+    step = 1
+    while step < rows:
+        inside = row >= step
+        before_decay = jnp.where(inside, pltpu.roll(decay, step, 0), 1.0)
+        before_state = jnp.where(inside, pltpu.roll(state, step, 0), 0.0)
+        state = state + decay * before_state
+        decay = decay * before_decay
+        step *= 2
+    return decay, state
+
+
+def recurrence_kernel(
+    rim_ref, signal_ref, kernel_ref, rec_ref, inp_ref, rate_ref, shift_ref,
+    prod_ref, state_ref, ext, diag_a, diag_b,
+):
+    rows, width = signal_ref.shape
+    taps = kernel_ref.shape[0]
+    lanes = diag_a.shape[0]
+    ext[0:8] = rim_ref[...].astype(jnp.float32)
+    ext[8 : 8 + rows] = signal_ref[...].astype(jnp.float32)
+    size = rec_ref.shape[1]
+    for c in range(width // lanes):
+        cols = slice(c * lanes, (c + 1) * lanes)
+        conv = kernel_ref[0:1, cols] * ext[9 - taps : 9 - taps + rows, cols]
+        for j in range(1, taps):
+            conv = conv + kernel_ref[j : j + 1, cols] * ext[9 - taps + j : 9 - taps + j + rows, cols]
+        conv = conv.astype(jnp.bfloat16)
+        per = lanes // size
+        rec = jax.nn.sigmoid(
+            jnp.dot(conv, block_diagonal(diag_a, rec_ref, c * per), preferred_element_type=jnp.float32)
+        )
+        inp = jax.nn.sigmoid(
+            jnp.dot(conv, block_diagonal(diag_b, inp_ref, c * per), preferred_element_type=jnp.float32)
+        )
+        log_decay = -RECURRENT_SCALE * rec * rate_ref[0:1, cols] + shift_ref[...]
+        driven = jnp.sqrt(-expm1_neg(2.0 * log_decay)) * inp * conv.astype(jnp.float32)
+        prod, state = scan_rows(jnp.exp(log_decay), driven)
+        prod_ref[:, cols] = prod
+        state_ref[:, cols] = state
 
 
 def rotate_half(values, token_positions):
@@ -53,10 +99,6 @@
 
 def rms_scaled(values, gain_vec):
     return values * lax.rsqrt(jnp.mean(values * values, axis=-1, keepdims=True) + EPS) * gain_vec
-
-
-def linear_step(earlier, later_part):
-    return (earlier[0] * later_part[0], later_part[0] * earlier[1] + later_part[1])
 
 
 def body(
@@ -93,58 +135,39 @@
     nope_width = head_dim - rope_width
     local_heads = query_width // head_dim
     head_value = value_width // local_heads
-    joined_weight = jnp.concatenate(
-        [recurrent_input, recurrent_gate, attention_gate, query_proj, latent_down, rope_key_down],
-        axis=1,
-    )
     normed = rms_scaled(
         lax.all_gather(tokens, "tp", axis=0, tiled=True).astype(jnp.float32), norm_gain
     ).astype(jnp.bfloat16)
-    projected = jnp.dot(normed, joined_weight, preferred_element_type=jnp.float32).astype(
-        jnp.bfloat16
-    )
-    local_tokens = projected.shape[0]
-    split_points = []
-    running_total = 0
-    for width_part in [channel_width, channel_width, value_width, query_width, latent_width]:
-        running_total += width_part
-        split_points.append(running_total)
-    recur_signal, recur_gate_pre, attention_pre, query_raw, latent_local, rope_raw = jnp.split(
-        projected, split_points, axis=1
-    )
+    recur_signal, recur_gate_pre, attention_pre, query_raw, latent_local, rope_raw = [
+        jnp.dot(normed, weight, preferred_element_type=jnp.float32).astype(jnp.bfloat16)
+        for weight in (
+            recurrent_input, recurrent_gate, attention_gate, query_proj, latent_down, rope_key_down,
+        )
+    ]
+    local_tokens = normed.shape[0]
     token_positions = sp_place * local_tokens + jnp.arange(local_tokens, dtype=jnp.int32)
     taps = conv_kernel.shape[0]
     conv_rim = from_behind(recur_signal[local_tokens - taps + 1 :], "sp", 1)
-    extended = jnp.concatenate([conv_rim, recur_signal], axis=0).astype(jnp.float32)
-    conv_sum = conv_kernel[0] * extended[0:local_tokens]
-    for tap_index in range(1, taps):
-        conv_sum = (
-            conv_sum + conv_kernel[tap_index] * extended[tap_index : tap_index + local_tokens]
-        )
-    conv_out = conv_sum.astype(jnp.bfloat16)
-    block_size = recurrence_gate_blocks.shape[1]
-    grouped = conv_out.reshape(local_tokens, channel_width // block_size, block_size)
-    recur_rate = jax.nn.sigmoid(
-        jnp.einsum(
-            "tbi,bij->tbj", grouped, recurrence_gate_blocks, preferred_element_type=jnp.float32
-        ).reshape(local_tokens, channel_width)
-    )
-    input_rate = jax.nn.sigmoid(
-        jnp.einsum(
-            "tbi,bij->tbj", grouped, input_gate_blocks, preferred_element_type=jnp.float32
-        ).reshape(local_tokens, channel_width)
-    )
-    log_decay = -RECURRENT_SCALE * recur_rate * decay_rate + decay_shift[:, None]
-    decay = jnp.exp(log_decay)
-    driven = jnp.sqrt(-jnp.expm1(2.0 * log_decay)) * input_rate * conv_out.astype(jnp.float32)
-    decay_prod, zero_state = lax.associative_scan(linear_step, (decay, driven), axis=0)
-    carry_decay, carry_state = prefix(
-        (decay_prod[-1], zero_state[-1]),
-        "sp",
-        linear_step,
-        (jnp.ones_like(initial_state), jnp.zeros_like(initial_state)),
-    )
-    incoming = carry_decay * initial_state + carry_state
+    rim8 = jnp.pad(conv_rim, ((8 - taps + 1, 0), (0, 0)))
+    lanes = min(128, channel_width)
+    shape = jax.ShapeDtypeStruct((local_tokens, channel_width), jnp.float32)
+    decay_prod, zero_state = pl.pallas_call(
+        recurrence_kernel,
+        out_shape=(shape, shape),
+        scratch_shapes=[
+            pltpu.VMEM((local_tokens + 8, channel_width), jnp.float32),
+            pltpu.VMEM((lanes, lanes), jnp.bfloat16),
+            pltpu.VMEM((lanes, lanes), jnp.bfloat16),
+        ],
+    )(
+        rim8, recur_signal, conv_kernel, recurrence_gate_blocks, input_gate_blocks,
+        decay_rate[None], decay_shift[:, None],
+    )
+    parts = lax.all_gather(jnp.stack([decay_prod[-1], zero_state[-1]]), "sp")
+    incoming = initial_state
+    for hop in range(sp_count - 1):
+        use = hop < sp_place
+        incoming = jnp.where(use, parts[hop, 0] * incoming + parts[hop, 1], incoming)
     states = zero_state + decay_prod * incoming
     recur_out = (states * jax.nn.silu(recur_gate_pre.astype(jnp.float32))).astype(jnp.bfloat16)
     query_rows = rms_scaled(

time: 531 us -> 132 us (0.25)
  the two profiles are of different devices: /device:TPU:0 before, /device:TPU:31 now
where the time goes in v1:
time: 132 us; the launch traced here: 130 us
  local copies, waits for them, and re-layouts  32.6 us (25%)
  matrix products  29.3 us (22%)
  waiting for transfers between devices  22.1 us (17%)
  other arithmetic  16.2 us (12%)
  between operations  13.4 us (10%)
  blocking collectives  10.5 us (8%)
  Pallas kernels  3.98 us (3%)
  starting transfers between devices  1.5 us (1%)
    unnamed x41, local copies, waits for them, and re-layouts  14.7 us
    reduce_scatter x1, waiting for transfers between devices, body(): lax.psum_scatter((jnp.dot(recur_out, recurrent_output, preferred_element_...  12.9 us
    all_gather x1, blocking collectives, body(): parts = lax.all_gather(jnp.stack([decay_prod[-1], zero_state[-1]]), 'sp')  10.5 us
    all_gather x1, waiting for transfers between devices, body(): lax.all_gather(tokens, 'tp', axis=0, tiled=True).astype(jnp.float32)  8.46 us
    reduce_sum x3, other arithmetic, rms_scaled(): jnp.mean(values * values, axis=-1, keepdims=True) + EPS  6.79 us
    dot_general x4, matrix products, body(): jnp.dot(normed, weight, preferred_element_type=jnp.float32)  6.49 us
    dot_general x1, matrix products, body(): jnp.dot(attention_out, attention_output, preferred_element_type=jnp.float32)  5.77 us
    dot_general x1, matrix products, body(): jnp.dot(recur_out, recurrent_output, preferred_element_type=jnp.float32)  5.73 us
  transfers between devices with their start and end apart: 4, of which 2 were waited for; matrix products, arithmetic and copies ran while one was open for 19% of the time, Pallas kernels for 3%

profile of v1, /device:TPU:31, one launch (start us, length us, event | category | flops | bytes accessed | tf_op | source)
XLA Modules:
  0.0 129.6 jit_solution(17200412927240083233)
XLA Ops:
  7.5 1.5 %copy.50.shift_ref = f32[256,1]{1,0:T(8,128)} copy(f32[256,1]{0,1:T(1,128)} %bitcast.66) | data formatting | bytes 2048 | tf_op jit(solution)/shard_map/broadcast_in_dim | solution.py:164
  11.1 8.5 %all-gather.5.cloned.1.call-done = bf16[256,2048]{1,0:T(8,128)(2,1)} async-done(((bf16[128,2048]{1,0:T(8,128)(2,1)}), bf16[256,2048]{1,0:T(8,128)(2,1)}) %all-gather.5.cloned.1.call-update) | async-done | bytes 1048592 | tf_op jit(solution)/shard_map/all_gather | solution.py:139
  19.6 1.7 %fusion.5 = f32[256]{0:T(256)S(1)} fusion(bf16[256,2048]{1,0:T(8,128)(2,1)} %all-gather.5.cloned.1.call-done), kind=kLoop, calls=%fused_computation.10 | loop fusion | flops 1572608 | bytes 1049600 | tf_op jit(solution)/shard_map/reduce_sum | solution.py:101
  21.3 1.8 %fusion.51 = bf16[256,64]{0,1:T(8,128)(2,1)S(1)} fusion(bf16[2048,64]{0,1:T(8,128)(2,1)} %param.26, bf16[256,2048]{1,0:T(8,128)(2,1)} %all-gather.5.cloned.1.call-done, f32[2048]{0:T(1024)S(1)} %copy-done.15, f32[256]{0:T(256)S(1)} %add_rsqrt_fusion.2), kind=kOutput, calls=%fused_computation.82 | convolution fusion | flops 69206016 | bytes 1352704 | tf_op jit(solution)/shard_map/dot_general | solution.py:142
  24.6 3.3 %fusion.11 = f32[256,768]{1,0:T(8,128)} fusion(bf16[2048,768]{1,0:T(8,128)(2,1)S(1)} %copy-done, bf16[256,2048]{1,0:T(8,128)(2,1)} %all-gather.5.cloned.1.call-done, f32[2048]{0:T(1024)S(1)} %copy-done.15, f32[256]{0:T(256)S(1)} %add_rsqrt_fusion.2), kind=kOutput, calls=%fused_computation.19 | convolution fusion | flops 807796736 | bytes 4989952 | tf_op jit(solution)/shard_map/dot_general | solution.py:142
  28.6 2.4 %copy.51 = f32[256,768]{0,1:T(8,128)} copy(f32[256,768]{1,0:T(8,128)} %fusion.11) | data formatting | bytes 1572864 | tf_op jit(solution)/shard_map/reshape | solution.py:174
  31.0 2.4 %copy.52 = f32[256,4,192]{2,0,1:T(8,128)} copy(f32[256,4,192]{0,2,1:T(8,128)} %bitcast.51) | data formatting | bytes 1572864 | tf_op jit(solution)/shard_map/reshape | solution.py:174
  33.5 1.4 %collective-permute-start = (bf16[3,512]{1,0:T(4,128)(2,1)S(1)}, bf16[3,512]{1,0:T(4,128)(2,1)S(1)}, u32[]{:S(2)}, u32[]{:S(2)}) collective-permute-start(bf16[3,512]{1,0:T(4,128)(2,1)S(1)} %slice.79), channel_id=1, source_target_pairs={{0,8},{8,16},{16,24},{1,9},{9,17},{17,25},{2,10},{10,18},{18,26},{... | collective-permute-start | bytes 9224 | tf_op jit(solution)/shard_map/ppermute | solution.py:18
  34.9 1.2 multiply_reduce_fusion.1
  36.2 1.4 %multiply_multiply_fusion = f32[256,4,192]{2,0,1:T(8,128)S(1)} fusion(f32[256,4,192]{2,0,1:T(8,128)} %copy.52, f32[192]{0:T(256)S(1)} %copy-done.10, f32[256,4]{0,1:T(4,128)S(1)} %add_rsqrt_fusion.1), kind=kLoop, calls=%fused_computation.34 | loop fusion | flops 393216 | bytes 1577728 | tf_op jit(solution)/shard_map/mul | solution.py:101
  40.2 4.0 %shard_map.181 = (f32[256,512]{1,0:T(8,128)}, f32[256,512]{1,0:T(8,128)}) custom-call(bf16[8,512]{1,0:T(8,128)(2,1)} %pad.4.rim_ref, bf16[256,512]{1,0:T(8,128)(2,1)} %copy-done.8, f32[4,512]{1,0:T(4,128)} %kernel_ref.1, bf16[8,64,64]{2,1,0:T(8,128)(2,1)} %rec_ref.1, bf16[8,64,64]{2,1,0:T(8,128)(2,1)} %inp_ref.1, f32[1,512]{1,0:T(1,128)} %bitcast.65, ...), custom_call_target="tpu_custom_call" | custom-call | tf_op jit(solution)/shard_map/pallas_call | solution.py:154
  45.6 10.5 %all-gather.1 = f32[4,2,512]{2,1,0:T(2,128)S(1)} all-gather(f32[1,2,512]{2,1,0:T(2,128)S(1)} %maximum_bitcast_fusion.2), channel_id=2, replica_groups=mesh['sp'=4,'fs'=4,'tp'=2] {'sp'}, dimensions={0}, use_global_device_ids=true | all-gather | bytes 20480 | tf_op jit(solution)/shard_map/all_gather | solution.py:166
  56.2 5.7 %fusion.28 = f32[256,2048]{1,0:T(8,128)} fusion(bf16[512,2048]{1,0:T(8,128)(2,1)} %param.36, f32[256,512]{1,0:T(8,128)} %get-tuple-element.29, f32[256,512]{1,0:T(8,128)} %get-tuple-element.30, bf16[2048,512]{1,0:T(8,128)(2,1)} %param.22, f32[512]{0:T(512)S(1)} %add_select_fusion, bf16[256,2048]{1,0:T(8,128)(2,1)} %all-gather.5.cloned.1.call-done, ...), kind=kOutput, calls=%fused_computation.42 | convolution fusion | flops 1077149696 | bytes 8399872 | tf_op jit(solution)/shard_map/dot_general | solution.py:248
  61.9 2.3 %slice.87 = bf16[256,4,2,256]{0,3,2,1:T(8,128)(2,1)} slice(bf16[256,4,2,288]{0,3,2,1:T(8,128)(2,1)} %bitcast.54), slice={[0:256], [0:4], [0:2], [0:256]} | slice | bytes 2097152 | tf_op jit(solution)/shard_map/slice | solution.py:188
  64.2 1.6 %slice_convert_fusion.2 = f32[256,4,2,32]{0,3,2,1:T(8,128)} fusion(bf16[256,4,2,288]{0,3,2,1:T(8,128)(2,1)} %bitcast.55), kind=kLoop, calls=%fused_computation.63 | loop fusion | flops 65536 | bytes 393216 | tf_op jit(solution)/shard_map/convert_element_type | solution.py:198
  65.8 3.7 %copy.66 = bf16[256,4,2,256]{3,2,1,0:T(2,128)(2,1)} copy(bf16[256,4,2,256]{0,3,2,1:T(8,128)(2,1)} %slice.87) | data formatting | bytes 2097152
  69.5 3.9 %multiply_reduce_fusion = f32[256,4]{1,0:T(8,128)S(1)} fusion(bf16[256,4,2,256]{3,2,1,0:T(2,128)(2,1)} %copy.66), kind=kLoop, calls=%fused_computation.16 | loop fusion | flops 1571840 | bytes 1052672 | tf_op jit(solution)/shard_map/reduce_sum | solution.py:101
  73.4 2.9 %copy.71 = f32[128,8,2,256]{3,1,2,0:T(8,128)} copy(bf16[128,8,2,256]{3,2,1,0:T(2,128)(2,1)} %bitcast.50) | data formatting | bytes 3145728
  76.4 3.3 %convolution_convert_fusion = bf16[1024,1024]{0,1:T(8,128)(2,1)S(1)} fusion(bf16[512,1024]{1,0:T(8,128)(2,1)} %param.34, f32[1024,512]{1,0:T(8,128)} %bitcast.53, f32[512]{0:T(512)} %param.33, f32[1024]{0:T(1024)S(1)} %rsqrt.30), kind=kOutput, calls=%fused_computation.17 | convolution fusion | flops 1076363264 | bytes 5249024 | tf_op jit(solution)/shard_map/dot_general | solution.py:195
  79.8 1.4 %copy-done.6 = bf16[1024,1024]{0,1:T(8,128)(2,1)} copy-done((bf16[1024,1024]{0,1:T(8,128)(2,1)}, bf16[1024,1024]{0,1:T(8,128)(2,1)S(1)}, u32[]{:S(2)}) %copy-start.6) | copy-done | bytes 2097176
  81.1 2.7 %fusion.24 = f32[4,256,1024]{2,1,0:T(8,128)} fusion(bf16[1024,4,256]{0,2,1:T(8,128)(2,1)S(1)} %bitcast.57, f32[256,4,192]{2,0,1:T(8,128)S(1)} %copy-done.2), kind=kOutput, calls=%fused_computation.30 | convolution fusion | flops 268435456 | bytes 5505024 | tf_op jit(solution)/shard_map/while/body/eval_jaxpr/thd,khd->htk/dot_general | solution.py:214
  83.8 2.1 %copy.73 = f32[256,4,2,32]{3,2,1,0:T(2,128)} copy(f32[256,4,2,32]{0,3,2,1:T(8,128)} %slice_convert_fusion.2) | data formatting | bytes 524288
  85.9 2.6 %reshape.189 = f32[1024,64]{1,0:T(8,128)} reshape(f32[256,4,2,32]{3,2,1,0:T(2,128)} %copy.73) | data formatting | bytes 524288 | tf_op jit(solution)/shard_map/convert_element_type | solution.py:198
  88.6 2.3 %fusion.58 = (f32[1024,32]{1,0:T(8,128)}, f32[1024,32]{1,0:T(8,128)}) fusion(f32[1024,64]{1,0:T(8,128)} %reshape.189), kind=kLoop, calls=%fused_computation.83 | loop fusion | bytes 524288 | tf_op jit(solution)/shard_map/slice | solution.py:90
  90.9 1.2 copy.69
  92.1 1.9 %copy.70 = f32[1024,32]{0,1:T(8,128)} copy(f32[1024,32]{1,0:T(8,128)} %get-tuple-element.33) | data formatting | bytes 262144
  94.0 1.5 %fusion.40 = (bf16[1024,32]{0,1:T(8,128)(2,1)S(1)}, bf16[1024,32]{0,1:T(8,128)(2,1)S(1)}) fusion(f32[1024,32]{0,1:T(8,128)} %copy.70, f32[1024,32]{0,1:T(8,128)S(1)} %copy.69, f32[32]{0:T(128)S(1)} %negate_power_fusion, f32[1024]{0:T(1024)S(1)} %convert_element_type.105), kind=kLoop, calls=%fused_computation.59 | loop fusion | flops 294912 | bytes 397440 | tf_op jit(solution)/shard_map/convert.3
  95.5 3.5 %fusion.60 = (f32[4,256]{1,0:T(4,128)S(1)}, f32[4,256,1024]{2,1,0:T(8,128)S(1)}) fusion(f32[4,256,1024]{2,1,0:T(8,128)} %fusion.24, bf16[256,4,32]{2,0,1:T(8,128)(2,1)} %get-tuple-element.32, bf16[256,4,32]{2,0,1:T(8,128)(2,1)S(1)} %get-tuple-element.31, bf16[1024,32]{0,1:T(8,128)(2,1)S(1)} %get-tuple-element.48, ...), kind=kOutput, calls=%fused_computation.85 | convolution fusion | flops 138935296 | bytes 8916992 | tf_op jit(solution)/shard_map/while/body/eval_jaxpr/thr,kr->htk/dot_general | solution.py:217
  100.6 1.8 %fusion.18 = f32[256,4,128]{0,2,1:T(8,128)} fusion(f32[4,256,1024]{2,1,0:T(8,128)S(1)} %get-tuple-element.60, f32[4,256]{1,0:T(4,128)S(1)} %get-tuple-element.59, bf16[1024,4,256]{0,2,1:T(8,128)(2,1)S(1)} %bitcast.58, f32[256,4]{0,1:T(4,128)S(1)} %bitcast_add_fusion.1, f32[256,4]{0,1:T(4,128)S(1)} %multiply_bitcast_fusion), kind=kOutput, calls=%fused_computation.22 | convolution fusion | flops 270794752 | bytes 5779456 | tf_op jit(solution)/shard_map/while/body/eval_jaxpr/htk,khd->thd/dot_general | solution.py:226
  102.4 2.0 %copy.65 = f32[256,512]{1,0:T(8,128)} copy(f32[256,512]{0,1:T(8,128)} %bitcast.56) | data formatting | bytes 1048576 | tf_op jit(solution)/shard_map/reshape | solution.py:244
  104.4 5.8 %fusion.4 = bf16[256,2048]{1,0:T(8,128)(2,1)} fusion(f32[256,2048]{1,0:T(8,128)} %fusion.28, bf16[512,2048]{1,0:T(8,128)(2,1)} %param.37, f32[256,512]{1,0:T(8,128)} %copy.65, bf16[2048,512]{1,0:T(8,128)(2,1)} %param.23, bf16[256,2048]{1,0:T(8,128)(2,1)} %all-gather.5.cloned.1.call-done, f32[2048]{0:T(1024)S(1)} %copy-done.17, f32[256]{0:T(256)S(1)} %copy-done.12), kind=kOutput, calls=%fused_computation.9 | convolution fusion | flops 1077936128 | bytes 8922112 | tf_op jit(solution)/shard_map/dot_general | solution.py:249
  110.2 12.9 %reduce-scatter.2.cloned.1.call-done = bf16[128,2048]{1,0:T(8,128)(2,1)} async-done(((bf16[256,2048]{1,0:T(8,128)(2,1)}), bf16[128,2048]{1,0:T(8,128)(2,1)}) %reduce-scatter.2.cloned.1.call-update) | async-done | bytes 524304 | tf_op jit(solution)/shard_map/reduce_scatter | solution.py:246
  (70 shorter events, 11.0 us)
Async XLA Ops:
  6.5 18.0 %copy-start = (bf16[2048,768]{1,0:T(8,128)(2,1)S(1)}, bf16[2048,768]{1,0:T(8,128)(2,1)}, u32[]{:S(2)}) copy-start(bf16[2048,768]{1,0:T(8,128)(2,1)} %param.24) | copy-start | bytes 9437188
  6.5 14.7 %copy-start.15 = (f32[2048]{0:T(1024)S(1)}, f32[2048]{0:T(1024)}, u32[]{:S(2)}) copy-start(f32[2048]{0:T(1024)} %param.20) | copy-start | bytes 24580
  6.5 13.0 %all-gather.5.cloned.1.call-start = ((), (), s32[]{:S(2)}) async-start(), calls=%async_computation.1 | async-start | bytes 1572864 | tf_op jit(solution)/shard_map/all_gather | solution.py:139
  7.3 54.6 %all-gather.7.cloned.1.call-start = ((), (), s32[]{:S(2)}) async-start(), calls=%async_computation.2 | async-start | bytes 1327104 | tf_op jit(solution)/shard_map/all_gather | solution.py:185
  19.6 3.5 %copy-start.3 = (bf16[256,2048]{1,0:T(8,128)(2,1)S(1)}, bf16[256,2048]{1,0:T(8,128)(2,1)}, u32[]{:S(2)}) copy-start(bf16[256,2048]{1,0:T(8,128)(2,1)} %all-gather.5.cloned.1.call-done) | copy-start | bytes 3145732
  19.6 3.5 %copy-start.14 = (bf16[2048,256]{1,0:T(8,128)(2,1)S(1)}, bf16[2048,256]{1,0:T(8,128)(2,1)}, u32[]{:S(2)}) copy-start(bf16[2048,256]{1,0:T(8,128)(2,1)} %param.25) | copy-start | bytes 3145732
  21.3 6.6 %copy-start.11 = (f32[256]{0:T(256)}, f32[256]{0:T(256)S(1)}, u32[]{:S(2)}) copy-start(f32[256]{0:T(256)S(1)} %add_rsqrt_fusion.2) | copy-start | bytes 3076
  24.5 98.6 %reduce-scatter.2.cloned.1.call-start = ((), (), s32[]{:S(2)}) async-start(), calls=%async_computation.3 | async-start | bytes 1572864 | tf_op jit(solution)/shard_map/reduce_scatter | solution.py:246
  24.5 3.3 %copy-start.4 = (bf16[256,2048]{1,0:T(8,128)(2,1)S(1)}, bf16[256,2048]{1,0:T(8,128)(2,1)}, u32[]{:S(2)}) copy-start(bf16[256,2048]{1,0:T(8,128)(2,1)} %all-gather.5.cloned.1.call-done) | copy-start | bytes 3145732
  24.5 3.3 %copy-start.13 = (bf16[2048,512]{1,0:T(8,128)(2,1)S(1)}, bf16[2048,512]{1,0:T(8,128)(2,1)}, u32[]{:S(2)}) copy-start(bf16[2048,512]{1,0:T(8,128)(2,1)} %param.21) | copy-start | bytes 6291460
  24.5 3.3 %copy-start.16 = (f32[2048]{0:T(1024)S(1)}, f32[2048]{0:T(1024)}, u32[]{:S(2)}) copy-start(f32[2048]{0:T(1024)} %param.20) | copy-start | bytes 24580
  28.6 7.5 %copy-start.8 = (bf16[256,512]{1,0:T(8,128)(2,1)}, bf16[256,512]{1,0:T(8,128)(2,1)S(1)}, u32[]{:S(2)}) copy-start(bf16[256,512]{1,0:T(8,128)(2,1)S(1)} %convolution_convert_fusion.4.signal_ref) | copy-start | bytes 786436
  28.6 7.5 %copy-start.10 = (f32[192]{0:T(256)S(1)}, f32[192]{0:T(256)}, u32[]{:S(2)}) copy-start(f32[192]{0:T(256)} %param.35) | copy-start | bytes 2308
  33.5 5.1 %copy-start.5 = (f32[256,32]{1,0:T(8,128)S(1)}, f32[256,32]{1,0:T(8,128)}, u32[]{:S(2)}) copy-start(f32[256,32]{1,0:T(8,128)} %get-tuple-element.58) | copy-start | bytes 98308
  33.5 6.1 %collective-permute-start = (bf16[3,512]{1,0:T(4,128)(2,1)S(1)}, bf16[3,512]{1,0:T(4,128)(2,1)S(1)}, u32[]{:S(2)}, u32[]{:S(2)}) collective-permute-start(bf16[3,512]{1,0:T(4,128)(2,1)S(1)} %slice.79), channel_id=1, source_target_pairs={{0,8},{8,16},{16,24},{1,9},{9,17},{17,25},{2,10},{10,18},{18,26},{... | collective-permute-start | bytes 9224 | tf_op jit(solution)/shard_map/ppermute | solution.py:18
  36.2 20.0 %copy-start.9 = (f32[512]{0:T(512)S(1)}, f32[512]{0:T(512)}, u32[]{:S(2)}) copy-start(f32[512]{0:T(512)} %param.32) | copy-start | bytes 6148
  37.6 1.0 copy-start.1
  37.6 18.5 %copy-start.12 = (f32[256]{0:T(256)S(1)}, f32[256]{0:T(256)}, u32[]{:S(2)}) copy-start(f32[256]{0:T(256)} %copy-done.11) | copy-start | bytes 3076
  76.4 4.7 %copy-start.2 = (f32[256,4,192]{2,0,1:T(8,128)S(1)}, f32[256,4,192]{2,0,1:T(8,128)}, u32[]{:S(2)}) copy-start(f32[256,4,192]{2,0,1:T(8,128)} %copy-done.1) | copy-start | bytes 2359300
  79.8 1.4 %copy-start.6 = (bf16[1024,1024]{0,1:T(8,128)(2,1)}, bf16[1024,1024]{0,1:T(8,128)(2,1)S(1)}, u32[]{:S(2)}) copy-start(bf16[1024,1024]{0,1:T(8,128)(2,1)S(1)} %convolution_convert_fusion) | copy-start | bytes 6291460
  99.0 1.6 %copy-start.7 = (bf16[1024,1024]{0,1:T(8,128)(2,1)S(1)}, bf16[1024,1024]{0,1:T(8,128)(2,1)}, u32[]{:S(2)}) copy-start(bf16[1024,1024]{0,1:T(8,128)(2,1)} %copy-done.6) | copy-start | bytes 6291460
  100.6 3.8 %copy-start.17 = (f32[2048]{0:T(1024)S(1)}, f32[2048]{0:T(1024)}, u32[]{:S(2)}) copy-start(f32[2048]{0:T(1024)} %param.20) | copy-start | bytes 24580
Sparse Core Ops, SparseCore 0:
  8.9 10.6 all-gather.4
  24.6 22.3 all-gather.6
  110.3 12.6 reduce-scatter.1

commit v2 on v1

v2 whole, which is shorter than its diff:
```python
import functools

import jax
import jax.numpy as jnp
import numpy as np
from jax import lax
from jax.experimental import pallas as pl
from jax.experimental.pallas import tpu as pltpu
from jax.sharding import PartitionSpec as P

EPS = 1e-06
RECURRENT_SCALE = 8.0
THETA = 10000.0
F32 = jnp.float32
BF16 = jnp.bfloat16
LANES = 128


def expm1_neg(y):
    small = y * (1.0 + y * (0.5 + y * (1.0 / 6 + y * (1.0 / 24 + y * (1.0 / 120 + y / 720)))))
    return jnp.where(y > -0.35, small, jnp.exp(y) - 1.0)


def block_diagonal(scratch, blocks_ref, first):
    size = blocks_ref.shape[1]
    scratch[...] = jnp.zeros_like(scratch)
    for k in range(scratch.shape[0] // size):
        scratch[k * size : (k + 1) * size, k * size : (k + 1) * size] = blocks_ref[first + k]
    return scratch[...]


def scan_rows(decay, state):
    rows = decay.shape[0]
    row = lax.broadcasted_iota(jnp.int32, decay.shape, 0)
    step = 1
    while step < rows:
        inside = row >= step
        before_decay = jnp.where(inside, pltpu.roll(decay, step, 0), 1.0)
        before_state = jnp.where(inside, pltpu.roll(state, step, 0), 0.0)
        state = state + decay * before_state
        decay = decay * before_decay
        step *= 2
    return decay, state


def rms_scaled(values, gain_vec):
    return values * lax.rsqrt(jnp.mean(values * values, axis=-1, keepdims=True) + EPS) * gain_vec


def rotary_tables(positions, width):
    half = width // 2
    inv_freq = (1.0 / THETA ** (np.arange(0, width, 2, dtype=np.float32) / width)).astype(np.float32)
    angles = np.arange(positions, dtype=np.float32)[:, None] * inv_freq[None, :]
    cosine = np.cos(angles.astype(np.float64)).astype(np.float32)
    sine = np.sin(angles.astype(np.float64)).astype(np.float32)
    return np.concatenate([cosine, cosine], 1), np.concatenate([-sine, sine], 1)


def rotate(values, cosine, sine):
    half = values.shape[-1] // 2
    swapped = jnp.concatenate([values[:, half:], values[:, :half]], axis=1)
    return values * cosine + swapped * sine


def column_step(width):
    return 256 if width % 256 == 0 else width


def remote(src, dst, send, recv, **where):
    return pltpu.make_async_remote_copy(
        src_ref=src, dst_ref=dst, send_sem=send, recv_sem=recv,
        device_id=where, device_id_type=pl.DeviceIdType.MESH,
    )


def layer_kernel(
    sp_count, tp_count,
    tokens, norm_gain, conv_kernel, rec_blocks, inp_blocks, decay_rate, decay_shift,
    initial_state, latent_gain, query_gain, cos_table, sin_table,
    h_lat, h_rope, h_in, h_gate, h_query, h_att, h_up, h_rout, h_aout,
    out,
    w_lat, w_rope, w_in, w_gate, w_query, w_att, w_up, w_rout, w_aout,
    tok_all, normed, lat_all, sig, gate, attp, qraw, rim_in, ext, diag_a, diag_b,
    prod, state, car_out, car_in, rout, racc, queries, kv, row_max, row_sum, acc, aout,
    part, part_in,
    w_sem, tok_s, tok_r, z_s, z_r, l_s, l_r, rim_s, rim_r, c_s, c_r, p_s, p_r,
):
    sp = lax.axis_index("sp")
    tp = lax.axis_index("tp")
    group = sp_count * tp_count
    share = tokens.shape[0]
    rows = normed.shape[0]
    taps, width = conv_kernel.shape
    head_dim = query_gain.shape[1]
    rope = w_rope.shape[1]
    nope = head_dim - rope
    heads = w_query.shape[1] // head_dim
    lat = w_lat.shape[1]
    value = attp.shape[1] // heads

    pairs = list(zip(
        (h_lat, h_rope, h_in, h_query, h_gate, h_att, h_up, h_rout, h_aout),
        (w_lat, w_rope, w_in, w_query, w_gate, w_att, w_up, w_rout, w_aout),
    ))
    loads = [pltpu.make_async_copy(a, b, w_sem.at[k]) for k, (a, b) in enumerate(pairs)]
    for load in loads:
        load.start()
    l_lat, l_rope, l_in, l_query, l_gate, l_att, l_up, l_rout, l_aout = loads

    barrier = pltpu.get_barrier_semaphore()

    def greet(d, carry):
        other = lax.rem(sp * tp_count + tp + d, group)
        pl.semaphore_signal(
            barrier, inc=1,
            device_id={"sp": other // tp_count, "tp": lax.rem(other, tp_count)},
            device_id_type=pl.DeviceIdType.MESH,
        )
        return carry

    lax.fori_loop(1, group, greet, 0)
    pl.semaphore_wait(barrier, group - 1)

    def peer(d):
        return lax.rem(tp + d, tp_count)

    def source(d):
        return lax.rem(tp - d + tp_count, tp_count)

    def token_copy(d):
        return remote(tokens, tok_all.at[d - 1], tok_s.at[d - 1], tok_r.at[d - 1], tp=peer(d))

    for d in range(1, tp_count):
        token_copy(d).start()

    def put_normed(block, place):
        normed[pl.ds(pl.multiple_of(place * share, share), share)] = rms_scaled(
            block.astype(F32), norm_gain[...]
        ).astype(BF16)

    put_normed(tokens[...], tp)
    for d in range(1, tp_count):
        token_copy(d).wait_recv()
        put_normed(tok_all[d - 1], source(d))

    def project(weight, into):
        step = column_step(weight.shape[1])
        for c in range(weight.shape[1] // step):
            cols = slice(c * step, (c + 1) * step)
            into[:, cols] = jnp.dot(
                normed[...], weight[:, cols], preferred_element_type=F32
            ).astype(BF16)

    l_lat.wait()
    l_rope.wait()
    own = lat_all.at[sp, tp]
    own[:, :lat] = jnp.dot(normed[...], w_lat[...], preferred_element_type=F32).astype(BF16)
    own[:, lat:] = jnp.dot(normed[...], w_rope[...], preferred_element_type=F32).astype(BF16)

    def along(e):
        block = lat_all.at[sp, tp]
        return remote(block, block, z_s.at[e - 1], z_r.at[e - 1], sp=sp + e)

    def landed(e):
        block = lat_all.at[sp - e, tp]
        return remote(block, block, z_s.at[e - 1], z_r.at[e - 1], sp=sp - e)

    def across(e, d):
        block = lat_all.at[sp - e, tp]
        return remote(block, block, l_s.at[e, d - 1], l_r.at[e, d - 1], tp=peer(d))

    def crossed(e, d):
        block = lat_all.at[sp - e, source(d)]
        return remote(block, block, l_s.at[e, d - 1], l_r.at[e, d - 1], tp=source(d))

    for e in range(1, sp_count):
        pl.when(sp + e < sp_count)(lambda e=e: along(e).start())
    for d in range(1, tp_count):
        across(0, d).start()

    l_in.wait()
    project(w_in, sig)

    def rim_copy():
        return remote(sig.at[pl.ds(rows - 16, 16)], rim_in, rim_s, rim_r, sp=sp + 1)

    def rim_landed():
        return remote(sig.at[pl.ds(rows - 16, 16)], rim_in, rim_s, rim_r, sp=sp - 1)

    pl.when(sp + 1 < sp_count)(lambda: rim_copy().start())

    @pl.when(sp == 0)
    def _():
        rim_in[...] = jnp.zeros_like(rim_in)

    l_query.wait()
    project(w_query, qraw)
    here = pl.ds(pl.multiple_of(sp * rows, rows), rows)
    for h in range(heads):
        head = rms_scaled(qraw[:, h * head_dim : (h + 1) * head_dim].astype(F32), query_gain[...])
        turned = rotate(head[:, nope:], cos_table[here], sin_table[here])
        queries[h, :, :nope] = head[:, :nope].astype(BF16)
        queries[h, :, nope:] = turned.astype(BF16)

    pl.when(sp > 0)(lambda: rim_landed().wait_recv())
    ext[0:8] = rim_in[8:16].astype(F32)
    ext[8 : 8 + rows] = sig[...].astype(F32)
    size = rec_blocks.shape[1]
    car_out[...] = jnp.zeros_like(car_out)
    shift = jnp.broadcast_to(decay_shift[...], (LANES, rows)).T
    for c in range(width // LANES):
        cols = slice(c * LANES, (c + 1) * LANES)
        conv = conv_kernel[0:1, cols] * ext[9 - taps : 9 - taps + rows, cols]
        for j in range(1, taps):
            first = 9 - taps + j
            conv = conv + conv_kernel[j : j + 1, cols] * ext[first : first + rows, cols]
        conv = conv.astype(BF16)
        per = LANES // size
        rec = jax.nn.sigmoid(
            jnp.dot(conv, block_diagonal(diag_a, rec_blocks, c * per), preferred_element_type=F32)
        )
        inp = jax.nn.sigmoid(
            jnp.dot(conv, block_diagonal(diag_b, inp_blocks, c * per), preferred_element_type=F32)
        )
        log_decay = -RECURRENT_SCALE * rec * decay_rate[0:1, cols] + shift
        driven = jnp.sqrt(-expm1_neg(2.0 * log_decay)) * inp * conv.astype(F32)
        one, two = scan_rows(jnp.exp(log_decay), driven)
        prod[:, cols] = one
        state[:, cols] = two
        car_out[0:1, cols] = one[rows - 1 :]
        car_out[1:2, cols] = two[rows - 1 :]

    def carry_copy(e):
        return remote(car_out, car_in.at[e - 1], c_s.at[e - 1], c_r.at[e - 1], sp=sp + e)

    def carry_landed(e):
        return remote(car_out, car_in.at[e - 1], c_s.at[e - 1], c_r.at[e - 1], sp=sp - e)

    for e in range(1, sp_count):
        pl.when(sp + e < sp_count)(lambda e=e: carry_copy(e).start())

    l_gate.wait()
    project(w_gate, gate)
    l_att.wait()
    project(w_att, attp)
    l_up.wait()

    for e in range(1, sp_count):

        @pl.when(sp >= e)
        def _(e=e):
            landed(e).wait_recv()
            for d in range(1, tp_count):
                across(e, d).start()

    scale = head_dim ** (-0.5)

    def attend(e, diagonal):
        place = sp - e
        blocks = [lat_all[place, n, :, :lat].astype(F32) for n in range(tp_count)]
        square = sum(jnp.sum(x * x, axis=-1, keepdims=True) for x in blocks)
        inverse = lax.rsqrt(square / (lat * tp_count) + EPS)
        total = None
        for n, x in enumerate(blocks):
            x = (x * inverse * latent_gain[0:1, n * lat : (n + 1) * lat]).astype(BF16)
            term = jnp.dot(x, w_up[n * lat : (n + 1) * lat], preferred_element_type=F32)
            total = term if total is None else total + term
        kv[...] = total.astype(BF16)
        there = pl.ds(pl.multiple_of(place * rows, rows), rows)
        turned = rotate(
            lat_all[place, tp, :, lat:].astype(F32), cos_table[there], sin_table[there]
        ).astype(BF16)
        for h in range(heads):
            base = h * (nope + value)
            keys = jnp.concatenate([kv[:, base : base + nope], turned], axis=1)
            scores = lax.dot_general(
                queries[h], keys, (((1,), (1,)), ((), ())), preferred_element_type=F32
            ) * scale
            if diagonal:
                seen = lax.broadcasted_iota(jnp.int32, scores.shape, 1)
                scores = jnp.where(
                    seen <= lax.broadcasted_iota(jnp.int32, scores.shape, 0), scores, -jnp.inf
                )
            top = jnp.max(scores, axis=-1, keepdims=True)
            if not diagonal:
                before = row_max[h, :, 0:1]
                top = jnp.maximum(top, before)
                fade = jnp.exp(before - top)
            weights = jnp.exp(scores - top)
            mass = jnp.sum(weights, axis=-1, keepdims=True)
            term = jnp.dot(
                weights.astype(BF16), kv[:, base + nope : base + nope + value],
                preferred_element_type=F32,
            )
            if not diagonal:
                mass = mass + row_sum[h, :, 0:1] * fade
                term = term + acc[h] * fade
            row_max[h] = jnp.broadcast_to(top, (rows, LANES))
            row_sum[h] = jnp.broadcast_to(mass, (rows, LANES))
            acc[h] = term

    for d in range(1, tp_count):
        crossed(0, d).wait_recv()
    attend(0, True)

    for e in range(1, sp_count):

        @pl.when(sp >= e)
        def _(e=e):
            carry_landed(e).wait_recv()

        @pl.when(sp < e)
        def _(e=e):
            car_in[e - 1, 0:1] = jnp.ones((1, width), F32)
            car_in[e - 1, 1:2] = jnp.zeros((1, width), F32)

    incoming = initial_state[...]
    for e in range(sp_count - 1, 0, -1):
        incoming = car_in[e - 1, 0:1] * incoming + car_in[e - 1, 1:2]
    for c in range(width // LANES):
        cols = slice(c * LANES, (c + 1) * LANES)
        full = state[:, cols] + prod[:, cols] * incoming[:, cols]
        rout[:, cols] = (full * jax.nn.silu(gate[:, cols].astype(F32))).astype(BF16)
    l_rout.wait()
    model = out.shape[1]
    step = column_step(model)
    for c in range(model // step):
        cols = slice(c * step, (c + 1) * step)
        racc[:, cols] = jnp.dot(rout[...], w_rout[:, cols], preferred_element_type=F32)

    def earlier(e, carry):
        for d in range(1, tp_count):
            crossed(e, d).wait_recv()
        attend(e, False)
        return carry

    lax.fori_loop(1, sp + 1, earlier, 0)
    for h in range(heads):
        cols = slice(h * value, (h + 1) * value)
        aout[:, cols] = (
            acc[h] / row_sum[h, :, 0:1] * jax.nn.silu(attp[:, cols].astype(F32))
        ).astype(BF16)
    l_aout.wait()
    for c in range(model // step):
        cols = slice(c * step, (c + 1) * step)
        both = racc[:, cols] + jnp.dot(aout[...], w_aout[:, cols], preferred_element_type=F32)
        part[:, :, cols] = both.astype(BF16).reshape(tp_count, share, step)

    def part_copy(d):
        return remote(part.at[peer(d)], part_in.at[d - 1], p_s.at[d - 1], p_r.at[d - 1], tp=peer(d))

    for d in range(1, tp_count):
        part_copy(d).start()
    for d in range(1, tp_count):
        part_copy(d).wait_recv()
    summed = part[tp].astype(F32)
    for d in range(1, tp_count):
        summed = summed + part_in[d - 1].astype(F32)
    out[...] = summed.astype(BF16)

    for d in range(1, tp_count):
        token_copy(d).wait_send()
        across(0, d).wait_send()
        part_copy(d).wait_send()
    pl.when(sp + 1 < sp_count)(lambda: rim_copy().wait_send())
    for e in range(1, sp_count):

        @pl.when(sp + e < sp_count)
        def _(e=e):
            along(e).wait_send()
            carry_copy(e).wait_send()

        @pl.when(sp >= e)
        def _(e=e):
            for d in range(1, tp_count):
                across(e, d).wait_send()


def body(
    tokens, norm_gain, recurrent_input, recurrent_gate, attention_gate, query_proj, latent_down,
    rope_key_down, conv_kernel, recurrence_gate_blocks, input_gate_blocks, decay_rate, decay_shift,
    initial_state, latent_gain, latent_up, query_gain, recurrent_output, attention_output,
):
    tp_count = lax.axis_size("tp")
    sp_count = lax.axis_size("sp")
    share, model = tokens.shape
    rows = share * tp_count
    width = recurrent_input.shape[1]
    taken = attention_gate.shape[1]
    head_dim = query_gain.shape[0]
    heads = query_proj.shape[1] // head_dim
    value = taken // heads
    lat = latent_down.shape[1]
    rope = rope_key_down.shape[1]
    cos_table, sin_table = rotary_tables(sp_count * rows, rope)
    hbm = [
        latent_down, rope_key_down, recurrent_input, recurrent_gate, query_proj, attention_gate,
        latent_up, recurrent_output, attention_output,
    ]
    small = [
        tokens, norm_gain[None], conv_kernel, recurrence_gate_blocks, input_gate_blocks,
        decay_rate[None], decay_shift[None], initial_state[None], latent_gain[None],
        query_gain[None], jnp.asarray(cos_table), jnp.asarray(sin_table),
    ]
    vmem = pltpu.VMEM
    dma = pltpu.SemaphoreType.DMA
    others = max(tp_count - 1, 1)
    hops = max(sp_count - 1, 1)
    return pl.pallas_call(
        functools.partial(layer_kernel, sp_count, tp_count),
        out_shape=jax.ShapeDtypeStruct((share, model), BF16),
        in_specs=[pl.BlockSpec(memory_space=pltpu.VMEM)] * len(small)
        + [pl.BlockSpec(memory_space=pl.ANY)] * len(hbm),
        out_specs=pl.BlockSpec(memory_space=pltpu.VMEM),
        scratch_shapes=[vmem(a.shape, a.dtype) for a in hbm]
        + [
            vmem((others, share, model), BF16),
            vmem((rows, model), BF16),
            vmem((sp_count, tp_count, rows, lat + rope), BF16),
            vmem((rows, width), BF16),
            vmem((rows, width), BF16),
            vmem((rows, taken), BF16),
            vmem((rows, query_proj.shape[1]), BF16),
            vmem((16, width), BF16),
            vmem((rows + 8, width), F32),
            vmem((LANES, LANES), BF16),
            vmem((LANES, LANES), BF16),
            vmem((rows, width), F32),
            vmem((rows, width), F32),
            vmem((8, width), F32),
            vmem((hops, 8, width), F32),
            vmem((rows, width), BF16),
            vmem((rows, model), F32),
            vmem((heads, rows, head_dim), BF16),
            vmem((rows, latent_up.shape[1]), BF16),
            vmem((heads, rows, LANES), F32),
            vmem((heads, rows, LANES), F32),
            vmem((heads, rows, value), F32),
            vmem((rows, taken), BF16),
            vmem((tp_count, share, model), BF16),
            vmem((others, share, model), BF16),
            dma((len(hbm),)),
            dma((others,)), dma((others,)),
            dma((hops,)), dma((hops,)),
            dma((sp_count, others)), dma((sp_count, others)),
            dma, dma,
            dma((hops,)), dma((hops,)),
            dma((others,)), dma((others,)),
        ],
        compiler_params=pltpu.CompilerParams(
            collective_id=0, has_side_effects=True, vmem_limit_bytes=60 * 1024 * 1024
        ),
    )(*small, *hbm)


def solution(mesh):
    return jax.shard_map(
        body,
        mesh=mesh,
        in_specs=(
            P(("fs", "sp", "tp"), None),
            P(),
            P(None, "tp"),
            P(None, "tp"),
            P(None, "tp"),
            P(None, "tp"),
            P(None, "tp"),
            P(),
            P(None, "tp"),
            P("tp", None, None),
            P("tp", None, None),
            P("tp"),
            P(("fs", "sp")),
            P(("fs", "tp")),
            P(),
            P(None, "tp"),
            P(),
            P("tp", None),
            P("tp", None),
        ),
        out_specs=P(("fs", "sp", "tp"), None),
        check_vma=False,
    )
```

time: 132 us -> 50.3 us (0.38); the launches traced: 130 us -> 50.1 us
  Pallas kernels: 3.98 us -> 46.2 us
  matrix products: 29.3 us -> 0 us
  local copies, waits for them, and re-layouts: 32.6 us -> 3.83 us
  waiting for transfers between devices: 22.1 us -> 0 us
  other arithmetic: 16.2 us -> 0 us
  between operations: 13.4 us -> 0.01 us
  blocking collectives: 10.5 us -> 0 us
  starting transfers between devices: 1.5 us -> 0 us
    pallas_call x1, Pallas kernels: 3.98 us -> 46.2 us  [body(): pl.pallas_call(functools.partial(layer_kernel, sp_count, tp_count), out_s...]
    dot_general x10 -> x0, matrix products: 29.3 us -> none  [the longest x4 6.49 us: body(): jnp.dot(normed, weight, preferred_element_type=jnp.float32)]
    reduce_scatter x1 -> x0, waiting for transfers between devices: 12.9 us -> none  [body(): lax.psum_scatter((jnp.dot(recur_out, recurrent_output, preferred_element_...]
    unnamed x41 -> x2, local copies, waits for them, and re-layouts: 14.7 us -> 3.83 us
    all_gather x1 -> x0, blocking collectives: 10.5 us -> none  [body(): parts = lax.all_gather(jnp.stack([decay_prod[-1], zero_state[-1]]), 'sp')]
    all_gather x2 -> x0, waiting for transfers between devices: 8.46 us -> none  [the longest x1 8.46 us: body(): lax.all_gather(tokens, 'tp', axis=0, tiled=True).astype(jnp.float32)]
    reduce_sum x4 -> x0, other arithmetic: 7.84 us -> none  [the longest x3 6.79 us: rms_scaled(): jnp.mean(values * values, axis=-1, keepdims=True) + EPS]
    reshape x3 -> x0, local copies, waits for them, and re-layouts: 6.89 us -> none  [the longest x2 4.84 us: body(): query_raw.astype(jnp.float32).reshape(local_tokens, local_heads, head_dim)]
  transfers between devices with their start and end apart: 4 -> 0, of which waited for: 2 -> 0; matrix products, arithmetic and copies ran while one was open for 19% -> 0% of each run, Pallas kernels for 3% -> 0%
where the time goes in v2:
time: 50.3 us; the launch traced here: 50.1 us
  Pallas kernels  46.2 us (92%)
  local copies, waits for them, and re-layouts  3.83 us (8%)
    pallas_call x1, Pallas kernels, body(): pl.pallas_call(functools.partial(layer_kernel, sp_count, tp_count), out_s...  46.2 us
    unnamed x2, local copies, waits for them, and re-layouts  3.83 us

profile of v2, /device:TPU:31, one launch (start us, length us, event | category | flops | bytes accessed | tf_op | source)
XLA Modules:
  0.0 50.1 jit_solution(14235971393368237541)
XLA Ops:
  0.0 2.0 %copy.22.h_rope = bf16[2048,64]{1,0:T(8,128)(2,1)} copy(bf16[2048,64]{0,1:T(8,128)(2,1)} %param.28) | data formatting | bytes 524288 | tf_op args[7]
  2.0 46.2 %shard_map.199 = bf16[128,2048]{1,0:T(8,128)(2,1)} custom-call(bf16[128,2048]{1,0:T(8,128)(2,1)} %tokens.1, f32[1,2048]{1,0:T(1,128)} %bitcast.6, f32[4,512]{1,0:T(4,128)} %conv_kernel.1, bf16[8,64,64]{2,1,0:T(8,128)(2,1)} %rec_blocks.1, bf16[8,64,64]{2,1,0:T(8,128)(2,1)} %inp_blocks.1, f32[1,512]{1,0:T(1,128)} %bitcast.7, f32[1,256]{1,0:T(1,128)} %bitcast.10, ...), custom_call_target="tpu_custom_call" | custom-call | tf_op jit(solution)/shard_map/pallas_call | solution.py:409
  48.2 1.9 %copy.24 = bf16[128,2048]{1,0:T(8,128)(2,1)} copy(bf16[128,2048]{1,0:T(8,128)(2,1)} %shard_map.199) | data formatting | bytes 1048576

commit v3 on v2

--- a/solution.py
+++ b/solution.py
@@ -92,20 +92,22 @@
     rows = normed.shape[0]
     taps, width = conv_kernel.shape
     head_dim = query_gain.shape[1]
-    rope = w_rope.shape[1]
+    rope = w_rope.shape[0]
     nope = head_dim - rope
     heads = w_query.shape[1] // head_dim
     lat = w_lat.shape[1]
     value = attp.shape[1] // heads
+    packed = lat // rope
+    tall = share // packed
 
     pairs = list(zip(
-        (h_lat, h_rope, h_in, h_query, h_gate, h_att, h_up, h_rout, h_aout),
-        (w_lat, w_rope, w_in, w_query, w_gate, w_att, w_up, w_rout, w_aout),
+        (h_in, h_lat, h_rope, h_query, h_gate, h_att, h_up, h_rout, h_aout),
+        (w_in, w_lat, w_rope, w_query, w_gate, w_att, w_up, w_rout, w_aout),
     ))
     loads = [pltpu.make_async_copy(a, b, w_sem.at[k]) for k, (a, b) in enumerate(pairs)]
     for load in loads:
         load.start()
-    l_lat, l_rope, l_in, l_query, l_gate, l_att, l_up, l_rout, l_aout = loads
+    l_in, l_lat, l_rope, l_query, l_gate, l_att, l_up, l_rout, l_aout = loads
 
     barrier = pltpu.get_barrier_semaphore()
 
@@ -151,19 +153,39 @@
                 normed[...], weight[:, cols], preferred_element_type=F32
             ).astype(BF16)
 
+    l_in.wait()
+    project(w_in, sig)
+
+    def rim_copy():
+        return remote(sig.at[pl.ds(rows - 16, 16)], rim_in, rim_s, rim_r, sp=sp + 1)
+
+    def rim_landed():
+        return remote(sig.at[pl.ds(rows - 16, 16)], rim_in, rim_s, rim_r, sp=sp - 1)
+
+    pl.when(sp + 1 < sp_count)(lambda: rim_copy().start())
+
+    @pl.when(sp == 0)
+    def _():
+        rim_in[...] = jnp.zeros_like(rim_in)
+
     l_lat.wait()
     l_rope.wait()
     own = lat_all.at[sp, tp]
-    own[:, :lat] = jnp.dot(normed[...], w_lat[...], preferred_element_type=F32).astype(BF16)
-    own[:, lat:] = jnp.dot(normed[...], w_rope[...], preferred_element_type=F32).astype(BF16)
+    own[:rows] = jnp.dot(normed[...], w_lat[...], preferred_element_type=F32).astype(BF16)
+    mine = normed[pl.ds(pl.multiple_of(tp * share, share), share)]
+    keyed = lax.dot_general(
+        mine, w_rope[...], (((1,), (1,)), ((), ())), preferred_element_type=F32
+    )
+    for k in range(packed):
+        own[rows:, k * rope : (k + 1) * rope] = keyed[k * tall : (k + 1) * tall].astype(BF16)
 
     def along(e):
-        block = lat_all.at[sp, tp]
-        return remote(block, block, z_s.at[e - 1], z_r.at[e - 1], sp=sp + e)
+        block = lat_all.at[sp - e, tp]
+        return remote(block, block, z_s.at[e], z_r.at[e], sp=sp + 1)
 
     def landed(e):
         block = lat_all.at[sp - e, tp]
-        return remote(block, block, z_s.at[e - 1], z_r.at[e - 1], sp=sp - e)
+        return remote(block, block, z_s.at[e - 1], z_r.at[e - 1], sp=sp - 1)
 
     def across(e, d):
         block = lat_all.at[sp - e, tp]
@@ -173,25 +195,19 @@
         block = lat_all.at[sp - e, source(d)]
         return remote(block, block, l_s.at[e, d - 1], l_r.at[e, d - 1], tp=source(d))
 
-    for e in range(1, sp_count):
-        pl.when(sp + e < sp_count)(lambda e=e: along(e).start())
+    if sp_count > 1:
+        pl.when(sp + 1 < sp_count)(lambda: along(0).start())
     for d in range(1, tp_count):
         across(0, d).start()
 
-    l_in.wait()
-    project(w_in, sig)
-
-    def rim_copy():
-        return remote(sig.at[pl.ds(rows - 16, 16)], rim_in, rim_s, rim_r, sp=sp + 1)
-
-    def rim_landed():
-        return remote(sig.at[pl.ds(rows - 16, 16)], rim_in, rim_s, rim_r, sp=sp - 1)
-
-    pl.when(sp + 1 < sp_count)(lambda: rim_copy().start())
-
-    @pl.when(sp == 0)
-    def _():
-        rim_in[...] = jnp.zeros_like(rim_in)
+    def relay(e):
+        @pl.when(sp >= e)
+        def _():
+            landed(e).wait_recv()
+            if e + 1 < sp_count:
+                pl.when(sp + 1 < sp_count)(lambda: along(e).start())
+            for d in range(1, tp_count):
+                across(e, d).start()
 
     l_query.wait()
     project(w_query, qraw)
@@ -202,6 +218,8 @@
         queries[h, :, :nope] = head[:, :nope].astype(BF16)
         queries[h, :, nope:] = turned.astype(BF16)
 
+    for e in range(1, min(2, sp_count)):
+        relay(e)
     pl.when(sp > 0)(lambda: rim_landed().wait_recv())
     ext[0:8] = rim_in[8:16].astype(F32)
     ext[8 : 8 + rows] = sig[...].astype(F32)
@@ -239,25 +257,22 @@
     for e in range(1, sp_count):
         pl.when(sp + e < sp_count)(lambda e=e: carry_copy(e).start())
 
+    for e in range(2, min(3, sp_count)):
+        relay(e)
     l_gate.wait()
     project(w_gate, gate)
     l_att.wait()
     project(w_att, attp)
     l_up.wait()
 
-    for e in range(1, sp_count):
-
-        @pl.when(sp >= e)
-        def _(e=e):
-            landed(e).wait_recv()
-            for d in range(1, tp_count):
-                across(e, d).start()
+    for e in range(3, sp_count):
+        relay(e)
 
     scale = head_dim ** (-0.5)
 
     def attend(e, diagonal):
         place = sp - e
-        blocks = [lat_all[place, n, :, :lat].astype(F32) for n in range(tp_count)]
+        blocks = [lat_all[place, n, :rows].astype(F32) for n in range(tp_count)]
         square = sum(jnp.sum(x * x, axis=-1, keepdims=True) for x in blocks)
         inverse = lax.rsqrt(square / (lat * tp_count) + EPS)
         total = None
@@ -267,9 +282,15 @@
             total = term if total is None else total + term
         kv[...] = total.astype(BF16)
         there = pl.ds(pl.multiple_of(place * rows, rows), rows)
-        turned = rotate(
-            lat_all[place, tp, :, lat:].astype(F32), cos_table[there], sin_table[there]
-        ).astype(BF16)
+        raw = jnp.concatenate(
+            [
+                lat_all[place, n, rows:, k * rope : (k + 1) * rope].astype(F32)
+                for n in range(tp_count)
+                for k in range(packed)
+            ],
+            axis=0,
+        )
+        turned = rotate(raw, cos_table[there], sin_table[there]).astype(BF16)
         for h in range(heads):
             base = h * (nope + value)
             keys = jnp.concatenate([kv[:, base : base + nope], turned], axis=1)
@@ -367,8 +388,11 @@
 
         @pl.when(sp + e < sp_count)
         def _(e=e):
-            along(e).wait_send()
             carry_copy(e).wait_send()
+
+        @pl.when((sp >= e - 1) & (sp + 1 < sp_count))
+        def _(e=e):
+            along(e - 1).wait_send()
 
         @pl.when(sp >= e)
         def _(e=e):
@@ -394,7 +418,7 @@
     rope = rope_key_down.shape[1]
     cos_table, sin_table = rotary_tables(sp_count * rows, rope)
     hbm = [
-        latent_down, rope_key_down, recurrent_input, recurrent_gate, query_proj, attention_gate,
+        latent_down, rope_key_down.T, recurrent_input, recurrent_gate, query_proj, attention_gate,
         latent_up, recurrent_output, attention_output,
     ]
     small = [
@@ -416,7 +440,7 @@
         + [
             vmem((others, share, model), BF16),
             vmem((rows, model), BF16),
-            vmem((sp_count, tp_count, rows, lat + rope), BF16),
+            vmem((sp_count, tp_count, rows + share * rope // lat, lat), BF16),
             vmem((rows, width), BF16),
             vmem((rows, width), BF16),
             vmem((rows, taken), BF16),

time: 50.3 us -> 40.9 us (0.81)
  Pallas kernels: 46.2 us -> 38.8 us
  local copies, waits for them, and re-layouts: 3.83 us -> 1.88 us
    pallas_call x1, Pallas kernels: 46.2 us -> 38.8 us  [body(): pl.pallas_call(functools.partial(layer_kernel, sp_count, tp_count), out_s...]
    unnamed x2 -> x1, local copies, waits for them, and re-layouts: 3.83 us -> 1.88 us
where the time goes in v3:
time: 40.9 us; the launch traced here: 40.7 us
  Pallas kernels  38.8 us (95%)
  local copies, waits for them, and re-layouts  1.88 us (5%)
    pallas_call x1, Pallas kernels, body(): pl.pallas_call(functools.partial(layer_kernel, sp_count, tp_count), out_s...  38.8 us
    unnamed x1, local copies, waits for them, and re-layouts  1.88 us

profile of v3, /device:TPU:31, one launch (start us, length us, event | category | flops | bytes accessed | tf_op | source)
XLA Modules:
  0.0 40.7 jit_solution(14688530649644917613)
XLA Ops:
  0.0 38.8 %shard_map.199 = bf16[128,2048]{1,0:T(8,128)(2,1)} custom-call(bf16[128,2048]{1,0:T(8,128)(2,1)} %tokens.1, f32[1,2048]{1,0:T(1,128)} %bitcast.8, f32[4,512]{1,0:T(4,128)} %conv_kernel.1, bf16[8,64,64]{2,1,0:T(8,128)(2,1)} %rec_blocks.1, bf16[8,64,64]{2,1,0:T(8,128)(2,1)} %inp_blocks.1, f32[1,512]{1,0:T(1,128)} %bitcast.9, f32[1,256]{1,0:T(1,128)} %bitcast.12, ...), custom_call_target="tpu_custom_call" | custom-call | tf_op jit(solution)/shard_map/pallas_call | solution.py:433
  38.9 1.9 %copy.23 = bf16[128,2048]{1,0:T(8,128)(2,1)} copy(bf16[128,2048]{1,0:T(8,128)(2,1)} %shard_map.199) | data formatting | bytes 1048576
